TPU v7x, 32 devices: a whole 2x2x4 slice. The times are simulated.
32 devices in a mesh: kv: 4 (over z), tp: 8 (over y, x, core).
Axes of the slice: x: 2, y: 2, z: 4, core: 2. Of those that a mesh axis runs over, the one named last changes fastest.
Arguments:
- piece_tokens: bfloat16 [512, 2048], P('kv'), may hold values from -6 to 6
- dec_tokens: bfloat16 [8, 2048], P('kv'), may hold values from -6 to 6
- norm_gain: float32 [2048], replicated, may hold values from 0.1 to 1.9
- w_query_nope: bfloat16 [2048, 2048], P(None, 'tp'), may hold values from -0.125 to 0.125
- w_query_rope: bfloat16 [2048, 1024], P(None, 'tp'), may hold values from -0.125 to 0.125
- w_latent: bfloat16 [2048, 512], replicated, may hold values from -0.125 to 0.125
- w_key_rope: bfloat16 [2048, 64], replicated, may hold values from -0.125 to 0.125
- latent_gain: float32 [512], replicated, may hold values from 0.1 to 1.9
- w_key_up: bfloat16 [16, 128, 512], P('tp'), may hold values from -0.5 to 0.5
- w_value_up: bfloat16 [16, 512, 128], P('tp'), may hold values from -3 to 3
- w_out: bfloat16 [2048, 2048], P(None, 'tp'), may hold values from -0.25 to 0.25
- prompt_latent: bfloat16 [2048, 512], P('kv'), may hold values from -210 to 210
- prompt_rope: bfloat16 [2048, 64], P('kv'), may hold values from -6 to 6
- dec_latent: bfloat16 [8, 1024, 512], P('kv'), may hold values from -210 to 210
- dec_rope: bfloat16 [8, 1024, 64], P('kv'), may hold values from -6 to 6
- dec_lengths: int32 [8], P('kv'), may hold values from 1 to 1024, 4096 in all
Outputs:
- piece_out: bfloat16 [512, 2048], P('kv', 'tp')
- dec_out: bfloat16 [8, 2048], P('kv', 'tp')
Inputs may be any that keep to these rules, and one draw needn't show every extreme that they name: `dec_lengths`: every decoding sequence has at least one live cache slot, and some sequence has all 1024.
All inputs are finite; a program needn't handle non-finite values. No bound on the sum of `dec_lengths` on one device may be relied on, other than what follows from the above.
Results may differ from a plain program's by a relative error of at most 0.025.
Values may be sent and summed in bfloat16 or wider, within the bound.
No kernel may reach another device: no remote copies, remote signals or barrier semaphores. Data moves between devices by JAX's collectives and lax.ppermute only.
A program may use at most 128 MiB of HBM per device.

v0:
```python
import jax
import jax.numpy as jnp
from jax import lax
from jax.sharding import PartitionSpec as P

epsilon = 1e-06
rope_base = 10000.0
masked = -1e30


def normalize(values, gain_vec):
    mean_sq = jnp.mean(values * values, axis=-1, keepdims=True)
    return values * lax.rsqrt(mean_sq + epsilon) * gain_vec


def rotate(values, positions):
    half_dim = values.shape[-1] // 2
    frequency = rope_base ** (-jnp.arange(half_dim, dtype=jnp.float32) / half_dim)
    angles = (positions.astype(jnp.float32)[:, None] * frequency[None, :])[:, None, :]
    cosines = jnp.cos(angles)
    sine_values = jnp.sin(angles)
    front_half = values[..., :half_dim]
    back_half = values[..., half_dim:]
    return jnp.concatenate(
        [
            front_half * cosines - back_half * sine_values,
            front_half * sine_values + back_half * cosines,
        ],
        axis=-1,
    )


def rounded(values):
    return lax.optimization_barrier(values.astype(jnp.bfloat16)).astype(jnp.float32)


def project(
    tokens, positions, norm_gain, w_query_nope, w_query_rope, w_latent, w_key_rope, latent_gain
):
    row_count = tokens.shape[0]
    rope_dim = w_key_rope.shape[1]
    head_count = w_query_rope.shape[1] // rope_dim
    normed = normalize(tokens.astype(jnp.float32), norm_gain).astype(jnp.bfloat16)
    query_nope = jnp.dot(normed, w_query_nope, preferred_element_type=jnp.float32).astype(
        jnp.bfloat16
    )
    query_raw = jnp.dot(normed, w_query_rope, preferred_element_type=jnp.float32).reshape(
        row_count, head_count, rope_dim
    )
    query_rot = rotate(query_raw, positions).astype(jnp.bfloat16)
    latent = normalize(
        jnp.dot(normed, w_latent, preferred_element_type=jnp.float32), latent_gain
    ).astype(jnp.bfloat16)
    key_raw = jnp.dot(normed, w_key_rope, preferred_element_type=jnp.float32)[:, None, :]
    key_rot = rotate(key_raw, positions)[:, 0].astype(jnp.bfloat16)
    return (query_nope, query_rot, latent, key_rot)


def absorb(query_nope, w_key_up):
    head_count, nope_dim, _ = w_key_up.shape
    by_head = query_nope.reshape(query_nope.shape[0], head_count, nope_dim)
    return jnp.einsum("nhd,hdc->nhc", by_head, w_key_up, preferred_element_type=jnp.float32).astype(
        jnp.bfloat16
    )


def shards(
    piece_tokens,
    dec_tokens,
    norm_gain,
    w_query_nope,
    w_query_rope,
    w_latent,
    w_key_rope,
    latent_gain,
    w_key_up,
    w_value_up,
    w_out,
    prompt_latent,
    prompt_rope,
    dec_latent,
    dec_rope,
    dec_lengths,
):
    piece_rows = piece_tokens.shape[0]
    dec_rows = dec_tokens.shape[0]
    cached = prompt_latent.shape[0]
    head_count, latent_dim, value_dim = w_value_up.shape
    rope_dim = w_key_rope.shape[1]
    nope_width = w_query_nope.shape[1]
    score_scale = (w_key_up.shape[1] + rope_dim) ** (-0.5)
    block_index = lax.axis_index("kv")
    prompt_len = cached * lax.axis_size("kv")
    piece_offset = block_index * piece_rows
    positions = jnp.concatenate(
        [prompt_len + piece_offset + jnp.arange(piece_rows, dtype=jnp.int32), dec_lengths]
    )
    tokens = jnp.concatenate([piece_tokens, dec_tokens], axis=0)
    query_nope, query_rot, new_latent, new_rot = project(
        tokens, positions, norm_gain, w_query_nope, w_query_rope, w_latent, w_key_rope, latent_gain
    )
    key_latent = jnp.concatenate([prompt_latent, new_latent[:piece_rows]], axis=0)
    key_rot = jnp.concatenate([prompt_rope, new_rot[:piece_rows]], axis=0)
    column = jnp.arange(key_latent.shape[0], dtype=jnp.int32)
    key_place = piece_offset + column - cached
    rot_width = head_count * rope_dim
    piece_rot = query_rot[:piece_rows].reshape(piece_rows, rot_width)
    outgoing = jnp.concatenate([query_nope[:piece_rows], piece_rot], axis=1)
    shard_rows = lax.all_gather(outgoing, "kv", axis=0, tiled=True)
    row_count = shard_rows.shape[0]
    query_lat = absorb(shard_rows[:, :nope_width], w_key_up)
    query_rope = shard_rows[:, nope_width:].reshape(row_count, head_count, rope_dim)
    score_row_count = query_lat.shape[0]
    scores = (
        jnp.einsum("qhc,kc->qhk", query_lat, key_latent, preferred_element_type=jnp.float32)
        + jnp.einsum("qhr,kr->qhk", query_rope, key_rot, preferred_element_type=jnp.float32)
    ) * score_scale
    query_place = jnp.arange(score_row_count, dtype=jnp.int32)
    visible = (column[None, :] < cached) | (key_place[None, :] <= query_place[:, None])
    scores = jnp.where(visible[:, None, :], scores, masked)
    row_peak = lax.pmax(jnp.max(scores, axis=2).astype(jnp.bfloat16), "kv").astype(jnp.float32)
    weights = jnp.exp(scores - row_peak[:, :, None])
    weight_sum = jnp.sum(weights, axis=2)
    mixed_lat = jnp.einsum(
        "qhk,kc->qhc", weights.astype(jnp.bfloat16), key_latent, preferred_element_type=jnp.float32
    ).astype(jnp.bfloat16)
    partial_value = jnp.einsum(
        "qhc,hcv->qhv", mixed_lat, w_value_up, preferred_element_type=jnp.float32
    )
    all_rows = partial_value.shape[0]
    partial_value = rounded(partial_value).reshape(all_rows, head_count * value_dim)
    summed, denominator = (
        lax.psum_scatter(
            partial_value.astype(jnp.bfloat16), "kv", scatter_dimension=0, tiled=True
        ).astype(jnp.float32),
        lax.psum_scatter(
            weight_sum.astype(jnp.bfloat16), "kv", scatter_dimension=0, tiled=True
        ).astype(jnp.float32),
    )
    piece_attn = (
        summed.reshape(piece_rows, head_count, value_dim) / denominator[:, :, None]
    ).astype(jnp.bfloat16)
    dec_query = absorb(query_nope[piece_rows:], w_key_up)
    dec_rot = query_rot[piece_rows:]
    own_lat = new_latent[piece_rows:]
    own_rot = new_rot[piece_rows:]
    cache_scores = (
        jnp.einsum("bhc,bkc->bhk", dec_query, dec_latent, preferred_element_type=jnp.float32)
        + jnp.einsum("bhr,bkr->bhk", dec_rot, dec_rope, preferred_element_type=jnp.float32)
    ) * score_scale
    live_keys = (
        jnp.arange(dec_latent.shape[1], dtype=jnp.int32)[None, None, :] < dec_lengths[:, None, None]
    )
    cache_scores = jnp.where(live_keys, cache_scores, masked)
    own_scores = (
        jnp.einsum("bhc,bc->bh", dec_query, own_lat, preferred_element_type=jnp.float32)
        + jnp.einsum("bhr,br->bh", dec_rot, own_rot, preferred_element_type=jnp.float32)
    ) * score_scale
    dec_peak = jnp.maximum(jnp.max(cache_scores, axis=2), own_scores)
    cache_w = jnp.exp(cache_scores - dec_peak[:, :, None])
    own_w = jnp.exp(own_scores - dec_peak)
    dec_sum = jnp.sum(cache_w, axis=2) + own_w
    dec_mix = (
        jnp.einsum(
            "bhk,bkc->bhc",
            cache_w.astype(jnp.bfloat16),
            dec_latent,
            preferred_element_type=jnp.float32,
        )
        + rounded(own_w)[:, :, None] * own_lat.astype(jnp.float32)[:, None, :]
    ).astype(jnp.bfloat16)
    dec_value = rounded(
        jnp.einsum("bhc,hcv->bhv", dec_mix, w_value_up, preferred_element_type=jnp.float32)
    )
    dec_attn = (dec_value / dec_sum[:, :, None]).astype(jnp.bfloat16)
    attended = jnp.concatenate(
        [
            piece_attn.reshape(piece_rows, head_count * value_dim),
            dec_attn.reshape(dec_rows, head_count * value_dim),
        ],
        axis=0,
    )
    result = jnp.dot(
        lax.all_gather(attended, "tp", axis=1, tiled=True),
        w_out,
        preferred_element_type=jnp.float32,
    ).astype(jnp.bfloat16)
    return (result[:piece_rows], result[piece_rows:])


def solution(mesh):
    in_specs = (
        P("kv", None),
        P("kv", None),
        P(),
        P(None, "tp"),
        P(None, "tp"),
        P(),
        P(),
        P(),
        P("tp", None, None),
        P("tp", None, None),
        P(None, "tp"),
        P("kv", None),
        P("kv", None),
        P("kv", None, None),
        P("kv", None, None),
        P("kv"),
    )
    out_specs = (P("kv", "tp"), P("kv", "tp"))
    return jax.shard_map(shards, mesh=mesh, in_specs=in_specs, out_specs=out_specs, check_vma=False)
```

profile of v0, /device:TPU:0, one launch (start us, length us, event | category | flops | bytes accessed | tf_op | source)
XLA Modules:
  0.0 113.8 jit_solution(15459763306817569072)
XLA Ops:
  7.3 1.4 %fusion.16 = f32[130]{0:T(256)S(1)} fusion(bf16[2,2048]{1,0:T(2,128)(2,1)} %param.17, bf16[128,2048]{1,0:T(8,128)(2,1)} %param.16), kind=kLoop, calls=%fused_computation.19 | loop fusion | flops 1597310 | bytes 533000 | tf_op jit(solution)/shard_map/reduce_sum | solution.py:12
  8.7 1.9 %convolution_convert_fusion.3 = bf16[130,256]{1,0:T(8,128)(2,1)S(1)} fusion(bf16[2048,256]{1,0:T(8,128)(2,1)} %param.19, f32[2048]{0:T(1024)} %param.18, f32[130]{0:T(256)S(1)} %add_rsqrt_fusion.1, bf16[2,2048]{1,0:T(2,128)(2,1)} %param.17, bf16[128,2048]{1,0:T(8,128)(2,1)} %param.16), kind=kOutput, calls=%fused_computation.17 | convolution fusion | flops 138211840 | bytes 1656328 | tf_op jit(solution)/shard_map/dot_general | solution.py:44
  11.2 0.6 multiply_reduce_fusion
  14.0 16.3 %all_gather.6 = bf16[512,384]{1,0:T(8,128)(2,1)S(1)} all-gather(bf16[128,384]{1,0:T(8,128)(2,1)S(1)} %pad_maximum_fusion.2), channel_id=1, replica_groups=mesh['kv'=4,'tp'=8] {'kv'}, dimensions={0}, use_global_device_ids=true | all-gather | bytes 491520 | tf_op jit(solution)/shard_map/all_gather | solution.py:109
  30.3 0.8 copy.47
  31.3 3.8 %fusion.3 = f32[512,2,640]{2,0,1:T(8,128)} fusion(bf16[2,128,512]{2,1,0:T(8,128)(2,1)S(1)} %copy-done.2, bf16[128,512]{1,0:T(8,128)(2,1)S(1)} %slice.76, bf16[512,512]{1,0:T(8,128)(2,1)} %param.27, bf16[512,384]{1,0:T(8,128)(2,1)S(1)} %all_gather.6), kind=kOutput, calls=%fused_computation.9 | convolution fusion | flops 807141376 | bytes 3801088 | tf_op jit(solution)/shard_map/qhc,kc->qhk/dot_general | solution.py:115
  35.1 4.2 %fusion.68 = (bf16[512,2]{0,1:T(2,128)(2,1)S(1)}, f32[512,2,640]{2,0,1:T(8,128)}) fusion(f32[512,2,640]{2,0,1:T(8,128)} %fusion.3, bf16[512,2,64]{0,2,1:T(8,128)(2,1)} %bitcast.72, bf16[128,64]{0,1:T(8,128)(2,1)S(1)} %fusion.40, bf16[512,64]{0,1:T(8,128)(2,1)} %param.28, pred[512,640]{1,0:T(8,128)(4,1)S(1)} %fusion.9), kind=kOutput, calls=%fused_computation.102 | convolution fusion | flops 86670336 | bytes 5785600 | tf_op jit(solution)/shard_map/qhr,kr->qhk/dot_general | solution.py:116
  39.3 12.4 %pmax.7 = bf16[512,2]{0,1:T(2,128)(2,1)S(1)} all-reduce(bf16[512,2]{0,1:T(2,128)(2,1)S(1)} %get-tuple-element.16), channel_id=1, replica_groups=mesh['kv'=4,'tp'=8] {'kv'}, use_global_device_ids=true, to_apply=%region_3.4 | all-reduce | flops 1024 | bytes 4096 | tf_op jit(solution)/shard_map/pmax | solution.py:121
  51.8 2.4 %fusion = bf16[512,2]{0,1:T(2,128)(2,1)S(1)} fusion(f32[512,2,640]{2,0,1:T(8,128)} %get-tuple-element.17, f32[512,2]{0,1:T(2,128)S(1)} %convert_element_type.109), kind=kLoop, calls=%fused_computation.2 | loop fusion | flops 1309696 | bytes 2627584 | tf_op jit(solution)/shard_map/reduce_sum | solution.py:123
  54.1 0.8 copy.61
  55.0 3.8 %fusion.13 = bf16[512,2,128]{2,0,1:T(8,128)(2,1)} fusion(bf16[2,512,128]{2,1,0:T(8,128)(2,1)} %param.25, f32[512,2,640]{2,0,1:T(8,128)} %get-tuple-element.17, f32[512,2]{0,1:T(2,128)S(1)} %convert_element_type.109, bf16[128,512]{1,0:T(8,128)(2,1)S(1)} %slice.76, bf16[512,512]{1,0:T(8,128)(2,1)S(1)} %copy-done.4), kind=kOutput, calls=%fused_computation.15 | convolution fusion | flops 808583168 | bytes 3805184 | tf_op jit(solution)/shard_map/qhc,hcv->qhv/dot_general | solution.py:127
  58.9 1.1 copy.48
  59.9 0.8 copy.59
  60.8 0.9 fusion.22
  62.0 2.2 %fusion.49 = f32[2,2,1024]{2,1,0:T(2,128)S(1)} fusion(bf16[2,1024,512]{2,1,0:T(8,128)(2,1)} %param.29, bf16[2,2,512]{2,0,1:T(2,128)(2,1)S(1)} %fusion.22), kind=kOutput, calls=%fused_computation.77 | convolution fusion | flops 4194304 | bytes 2117632 | tf_op jit(solution)/shard_map/bhc,bkc->bhk/dot_general | solution.py:148
  65.0 2.0 %fusion.21 = bf16[2,2,512]{2,1,0:T(2,128)(2,1)S(1)} fusion(bf16[2,1024,512]{2,1,0:T(8,128)(2,1)} %param.29, f32[2,2,1024]{2,1,0:T(2,128)S(1)} %get-tuple-element.13, f32[2,2]{1,0:T(2,128)S(1)} %fusion.55, f32[2,512]{1,0:T(2,128)S(1)} %get-tuple-element.6, f32[2,2]{1,0:T(2,128)S(1)} %convert_element_type.123), kind=kOutput, calls=%fused_computation.26 | convolution fusion | flops 4208640 | bytes 2121760 | tf_op jit(solution)/shard_map/bhk,bkc->bhc/dot_general | solution.py:164
  67.5 5.3 %reduce-scatter.9.cloned.1.call-done = bf16[128,2]{1,0:T(8,128)(2,1)} async-done(((bf16[512,2]{1,0:T(8,128)(2,1)}), bf16[128,2]{1,0:T(8,128)(2,1)}) %reduce-scatter.9.cloned.1.call-update) | async-done | bytes 528
  72.8 0.8 copy.62
  73.6 19.7 %reduce-scatter.7.cloned.1.call-done = bf16[128,256]{1,0:T(8,128)(2,1)} async-done(((bf16[512,256]{1,0:T(8,128)(2,1)}), bf16[128,256]{1,0:T(8,128)(2,1)}) %reduce-scatter.7.cloned.1.call-update) | async-done | bytes 65552
  93.3 0.9 copy.60
  94.3 10.9 %all_gather.7 = bf16[130,2048]{0,1:T(8,128)(2,1)S(1)} all-gather(bf16[130,256]{0,1:T(8,128)(2,1)S(1)} %pad_maximum_fusion.1), channel_id=1, replica_groups=mesh['kv'=4,'tp'=8] {'tp'}, dimensions={1}, use_global_device_ids=true | all-gather | bytes 599040 | tf_op jit(solution)/shard_map/all_gather | solution.py:184
  105.2 0.5 convolution_convert_fusion.2
  105.7 0.6 slice.84
  106.4 0.6 slice.85
  (75 shorter events, 4.6 us)
Async XLA Ops:
  7.2 4.0 %copy-start = (bf16[2048,512]{1,0:T(8,128)(2,1)S(1)}, bf16[2048,512]{1,0:T(8,128)(2,1)}, u32[]{:S(2)}) copy-start(bf16[2048,512]{1,0:T(8,128)(2,1)} %param.21) | copy-start | bytes 6291460
  7.2 65.6 %reduce-scatter.9.cloned.1.call-start = ((), (), s32[]{:S(2)}) async-start(), calls=%async_computation.3 | async-start | bytes 163840
  8.6 1.9 %copy-start.3 = (bf16[128,2048]{1,0:T(8,128)(2,1)S(1)}, bf16[128,2048]{1,0:T(8,128)(2,1)}, u32[]{:S(2)}) copy-start(bf16[128,2048]{1,0:T(8,128)(2,1)} %param.16) | copy-start | bytes 1572868
  8.7 1.9 %copy-start.7 = (bf16[2,2048]{1,0:T(2,128)(2,1)S(1)}, bf16[2,2048]{1,0:T(2,128)(2,1)}, u32[]{:S(2)}) copy-start(bf16[2,2048]{1,0:T(2,128)(2,1)} %param.17) | copy-start | bytes 24580
  8.7 1.9 %copy-start.10 = (bf16[2048,128]{1,0:T(8,128)(2,1)S(1)}, bf16[2048,128]{1,0:T(8,128)(2,1)}, u32[]{:S(2)}) copy-start(bf16[2048,128]{1,0:T(8,128)(2,1)} %param.20) | copy-start | bytes 1572868
  8.7 1.9 %copy-start.13 = (f32[2048]{0:T(1024)S(1)}, f32[2048]{0:T(1024)}, u32[]{:S(2)}) copy-start(f32[2048]{0:T(1024)} %param.18) | copy-start | bytes 24580
  10.6 3.4 %copy-start.6 = (bf16[130,256]{1,0:T(8,128)(2,1)}, bf16[130,256]{1,0:T(8,128)(2,1)S(1)}, u32[]{:S(2)}) copy-start(bf16[130,256]{1,0:T(8,128)(2,1)S(1)} %convolution_convert_fusion.3) | copy-start | bytes 199684
  11.2 1.0 copy-start.11
  11.8 0.8 copy-start.9
  11.8 1.3 %copy-start.8 = (f32[512]{0:T(512)S(1)}, f32[512]{0:T(512)}, u32[]{:S(2)}) copy-start(f32[512]{0:T(512)} %param.23) | copy-start | bytes 6148
  13.2 18.1 %copy-start.2 = (bf16[2,128,512]{2,1,0:T(8,128)(2,1)S(1)}, bf16[2,128,512]{2,1,0:T(8,128)(2,1)}, u32[]{:S(2)}) copy-start(bf16[2,128,512]{2,1,0:T(8,128)(2,1)} %param.24) | copy-start | bytes 786436
  51.7 3.3 %copy-start.4 = (bf16[512,512]{1,0:T(8,128)(2,1)S(1)}, bf16[512,512]{1,0:T(8,128)(2,1)}, u32[]{:S(2)}) copy-start(bf16[512,512]{1,0:T(8,128)(2,1)} %param.27) | copy-start | bytes 1572868
  55.0 38.3 %reduce-scatter.7.cloned.1.call-start = ((), (), s32[]{:S(2)}) async-start(), calls=%async_computation.2 | async-start | bytes 327680
  60.8 3.7 %copy-start.12 = (bf16[2,1024,64]{1,2,0:T(8,128)(2,1)S(1)}, bf16[2,1024,64]{1,2,0:T(8,128)(2,1)}, u32[]{:S(2)}) copy-start(bf16[2,1024,64]{1,2,0:T(8,128)(2,1)} %param.30) | copy-start | bytes 786436
  64.2 2.8 %copy-start.5 = (bf16[2,512,128]{2,1,0:T(8,128)(2,1)S(1)}, bf16[2,512,128]{2,1,0:T(8,128)(2,1)}, u32[]{:S(2)}) copy-start(bf16[2,512,128]{2,1,0:T(8,128)(2,1)} %param.25) | copy-start | bytes 786436
  67.0 38.2 %copy-start.1 = (bf16[2048,256]{1,0:T(8,128)(2,1)S(1)}, bf16[2048,256]{1,0:T(8,128)(2,1)}, u32[]{:S(2)}) copy-start(bf16[2048,256]{1,0:T(8,128)(2,1)} %param.26) | copy-start | bytes 3145732
Sparse Core Ops, SparseCore 0:
  55.1 17.6 reduce-scatter.8
  75.1 18.2 reduce-scatter.6
where the time goes:
time: 114 us
  blocking collectives  39.6 us (35%)
  waiting for transfers between devices  25 us (22%)
  matrix products  21.3 us (19%)
  between operations  14.4 us (13%)
  local copies, waits for them, and re-layouts  7.52 us (7%)
  other arithmetic  5.78 us (5%)
    unnamed x4, waiting for transfers between devices  25 us
    all_gather x1, blocking collectives, shards(): shard_rows = lax.all_gather(outgoing, 'kv', axis=0, tiled=True)  16.3 us
    pmax x1, blocking collectives, shards(): lax.pmax(jnp.max(scores, axis=2).astype(jnp.bfloat16), 'kv')  12.4 us
    all_gather x1, blocking collectives, shards(): lax.all_gather(attended, 'tp', axis=1, tiled=True)  10.9 us
    dot_general x1, matrix products, shards(): jnp.einsum('qhr,kr->qhk', query_rope, key_rot, preferred_element_type=jnp...  4.18 us
    dot_general x1, matrix products, shards(): jnp.einsum('qhc,hcv->qhv', mixed_lat, w_value_up, preferred_element_type=...  3.83 us
    dot_general x1, matrix products, shards(): jnp.einsum('qhc,kc->qhk', query_lat, key_latent, preferred_element_type=j...  3.79 us
    unnamed x32, local copies, waits for them, and re-layouts  3.78 us
  transfers between devices with their start and end apart: 2, of which 2 were waited for; matrix products, arithmetic and copies ran while one was open for 12% of the time, Pallas kernels for 0%

commit v1 on v0

--- a/solution.py
+++ b/solution.py
@@ -106,7 +106,12 @@
     rot_width = head_count * rope_dim
     piece_rot = query_rot[:piece_rows].reshape(piece_rows, rot_width)
     outgoing = jnp.concatenate([query_nope[:piece_rows], piece_rot], axis=1)
-    shard_rows = lax.all_gather(outgoing, "kv", axis=0, tiled=True)
+    ring = [outgoing]
+    for hop in range(3):
+        ring.append(lax.ppermute(ring[-1], "kv", [(dev, (dev + 1) % 4) for dev in range(4)]))
+    shard_rows = jnp.roll(
+        jnp.concatenate(ring[::-1], axis=0), (lax.axis_index("kv") + 1) * ring[0].shape[0], axis=0
+    )
     row_count = shard_rows.shape[0]
     query_lat = absorb(shard_rows[:, :nope_width], w_key_up)
     query_rope = shard_rows[:, nope_width:].reshape(row_count, head_count, rope_dim)

time: 114 us -> 123 us (1.079)
  blocking collectives: 39.6 us -> 19.2 us
  waiting for transfers between devices: 25 us -> 42 us
  other arithmetic: 5.78 us -> 11 us
  starting transfers between devices: 0.08 us -> 4.71 us
  local copies, waits for them, and re-layouts: 7.52 us -> 11.4 us
  matrix products: 21.3 us -> 19.1 us
    all_gather x1 -> x0, blocking collectives: 16.3 us -> none  [shards(): shard_rows = lax.all_gather(outgoing, 'kv', axis=0, tiled=True)]
    ppermute x0 -> x3, waiting for transfers between devices: none -> 9.83 us  [shards(): lax.ppermute(ring[-1], 'kv', [(dev, (dev + 1) % 4) for dev in range(4)])]
    unnamed x4, waiting for transfers between devices: 25 us -> 32.2 us
    unnamed x32 -> x68, local copies, waits for them, and re-layouts: 3.78 us -> 8.59 us
    ppermute x0 -> x3, starting transfers between devices: none -> 4.63 us  [shards(): lax.ppermute(ring[-1], 'kv', [(dev, (dev + 1) % 4) for dev in range(4)])]
    pmax x1, blocking collectives: 12.4 us -> 8.35 us  [shards(): lax.pmax(jnp.max(scores, axis=2).astype(jnp.bfloat16), 'kv')]
    dot_general x1, matrix products: 2.23 us -> 0.64 us  [shards(): jnp.einsum('bhc,bkc->bhk', dec_query, dec_latent, preferred_element_type=...]
  transfers between devices with their start and end apart: 2 -> 5, of which waited for: 2 -> 4; matrix products, arithmetic and copies ran while one was open for 12% -> 12% of each run, Pallas kernels for 0% -> 0%
where the time goes in v1:
time: 123 us; the launch traced here: 122 us
  waiting for transfers between devices  42 us (34%)
  blocking collectives  19.2 us (16%)
  matrix products  19.1 us (16%)
  between operations  14.5 us (12%)
  local copies, waits for them, and re-layouts  11.4 us (9%)
  other arithmetic  11 us (9%)
  starting transfers between devices  4.71 us (4%)
    unnamed x4, waiting for transfers between devices  32.2 us
    all_gather x1, blocking collectives, shards(): lax.all_gather(attended, 'tp', axis=1, tiled=True)  10.9 us
    ppermute x3, waiting for transfers between devices, shards(): lax.ppermute(ring[-1], 'kv', [(dev, (dev + 1) % 4) for dev in range(4)])  9.83 us
    unnamed x68, local copies, waits for them, and re-layouts  8.59 us
    pmax x1, blocking collectives, shards(): lax.pmax(jnp.max(scores, axis=2).astype(jnp.bfloat16), 'kv')  8.35 us
    ppermute x3, starting transfers between devices, shards(): lax.ppermute(ring[-1], 'kv', [(dev, (dev + 1) % 4) for dev in range(4)])  4.63 us
    dot_general x1, matrix products, shards(): jnp.einsum('qhr,kr->qhk', query_rope, key_rot, preferred_element_type=jnp...  4.05 us
    dot_general x1, matrix products, shards(): jnp.einsum('qhc,kc->qhk', query_lat, key_latent, preferred_element_type=j...  3.72 us
  transfers between devices with their start and end apart: 5, of which 4 were waited for; matrix products, arithmetic and copies ran while one was open for 12% of the time, Pallas kernels for 0%

profile of v1, /device:TPU:0, one launch (start us, length us, event | category | flops | bytes accessed | tf_op | source)
XLA Modules:
  0.0 121.9 jit_solution(7328725645374800780)
XLA Ops:
  7.2 1.4 %fusion.16 = f32[130]{0:T(256)S(1)} fusion(bf16[2,2048]{1,0:T(2,128)(2,1)} %param.17, bf16[128,2048]{1,0:T(8,128)(2,1)} %param.16), kind=kLoop, calls=%fused_computation.19 | loop fusion | flops 1597310 | bytes 533000 | tf_op jit(solution)/shard_map/reduce_sum | solution.py:12
  8.7 1.9 %convolution_convert_fusion.3 = bf16[130,256]{1,0:T(8,128)(2,1)S(1)} fusion(bf16[2048,256]{1,0:T(8,128)(2,1)} %param.19, f32[2048]{0:T(1024)} %param.18, f32[130]{0:T(256)S(1)} %add_rsqrt_fusion.1, bf16[2,2048]{1,0:T(2,128)(2,1)} %param.17, bf16[128,2048]{1,0:T(8,128)(2,1)} %param.16), kind=kOutput, calls=%fused_computation.17 | convolution fusion | flops 138211840 | bytes 1656328 | tf_op jit(solution)/shard_map/dot_general | solution.py:44
  13.0 3.0 %collective-permute-start = (bf16[128,384]{1,0:T(8,128)(2,1)}, bf16[128,384]{1,0:T(8,128)(2,1)}, u32[]{:S(2)}, u32[]{:S(2)}) collective-permute-start(bf16[128,384]{1,0:T(8,128)(2,1)} %pad_maximum_fusion.2), channel_id=1, source_target_pairs={{0,8},{8,16},{16,24},{24,0},{1,9},{9,17},{17,25},{25,1},{2,10},{10... | collective-permute-start | bytes 294920 | tf_op jit(solution)/shard_map/ppermute | solution.py:111
  20.7 1.2 fusion.67
  22.1 1.6 %collective-permute-start.1 = (bf16[128,384]{1,0:T(8,128)(2,1)}, bf16[128,384]{1,0:T(8,128)(2,1)}, u32[]{:S(2)}, u32[]{:S(2)}) collective-permute-start(bf16[128,384]{1,0:T(8,128)(2,1)} %collective-permute-done), channel_id=1, source_target_pairs={{0,8},{8,16},{16,24},{24,0},{1,9},{9,17},{17,25},{25,1},{2,10},{10... | collective-permute-start | bytes 294920 | tf_op jit(solution)/shard_map/ppermute | solution.py:111
  24.9 3.9 %collective-permute-done.1 = bf16[128,384]{1,0:T(8,128)(2,1)} collective-permute-done((bf16[128,384]{1,0:T(8,128)(2,1)}, bf16[128,384]{1,0:T(8,128)(2,1)}, u32[]{:S(2)}, u32[]{:S(2)}) %collective-permute-start.1) | collective-permute-done | bytes 98336 | tf_op jit(solution)/shard_map/ppermute | solution.py:111
  29.5 5.9 %collective-permute-done.2 = bf16[128,384]{1,0:T(8,128)(2,1)S(1)} collective-permute-done((bf16[128,384]{1,0:T(8,128)(2,1)}, bf16[128,384]{1,0:T(8,128)(2,1)S(1)}, u32[]{:S(2)}, u32[]{:S(2)}) %collective-permute-start.2) | collective-permute-done | bytes 98336 | tf_op jit(solution)/shard_map/ppermute | solution.py:111
  35.5 0.9 constant_dynamic-update-slice_fusion.6
  36.4 0.9 constant_dynamic-update-slice_fusion.5
  38.1 0.9 constant_dynamic-update-slice_fusion.2
  39.0 0.9 constant_dynamic-update-slice_fusion.1
  40.7 0.9 copy-done.8
  42.4 3.7 %fusion.3 = f32[512,2,640]{2,0,1:T(8,128)} fusion(bf16[2,128,512]{2,1,0:T(8,128)(2,1)S(1)} %copy-done.2, bf16[128,512]{1,0:T(8,128)(2,1)S(1)} %slice.75, bf16[512,512]{1,0:T(8,128)(2,1)S(1)} %copy-done.5, bf16[1024,384]{1,0:T(8,128)(2,1)} %copy-done.8, s32[]{:T(128)S(6)} %select_n.22), kind=kOutput, calls=%fused_computation.9 | convolution fusion | flops 807141376 | bytes 3801092 | tf_op jit(solution)/shard_map/qhc,kc->qhk/dot_general | solution.py:120
  46.1 4.0 %fusion.68 = (bf16[512,2]{0,1:T(2,128)(2,1)S(1)}, f32[512,2,640]{2,0,1:T(8,128)}) fusion(f32[512,2,640]{2,0,1:T(8,128)} %fusion.3, bf16[512,2,64]{0,2,1:T(8,128)(2,1)S(1)} %bitcast.72, bf16[128,64]{0,1:T(8,128)(2,1)S(1)} %fusion.40, bf16[512,64]{0,1:T(8,128)(2,1)S(1)} %copy-done.14, pred[512,640]{1,0:T(8,128)(4,1)S(1)} %fusion.9), kind=kOutput, calls=%fused_computation.110 | convolution fusion | flops 86670336 | bytes 5785600 | tf_op jit(solution)/shard_map/qhr,kr->qhk/dot_general | solution.py:121
  50.2 8.3 %pmax.7 = bf16[512,2]{0,1:T(2,128)(2,1)S(1)} all-reduce(bf16[512,2]{0,1:T(2,128)(2,1)S(1)} %get-tuple-element.16), channel_id=1, replica_groups=mesh['kv'=4,'tp'=8] {'kv'}, use_global_device_ids=true, to_apply=%region_3.4 | all-reduce | flops 1024 | bytes 4096 | tf_op jit(solution)/shard_map/pmax | solution.py:126
  58.5 2.4 %fusion = bf16[512,2]{0,1:T(2,128)(2,1)S(1)} fusion(f32[512,2,640]{2,0,1:T(8,128)} %get-tuple-element.17, f32[512,2]{0,1:T(2,128)S(1)} %convert_element_type.109), kind=kLoop, calls=%fused_computation.2 | loop fusion | flops 1309696 | bytes 2627584 | tf_op jit(solution)/shard_map/reduce_sum | solution.py:128
  61.8 3.1 %fusion.13 = bf16[512,2,128]{2,0,1:T(8,128)(2,1)S(1)} fusion(bf16[2,512,128]{2,1,0:T(8,128)(2,1)S(1)} %copy-done.9, f32[512,2,640]{2,0,1:T(8,128)} %get-tuple-element.17, f32[512,2]{0,1:T(2,128)S(1)} %convert_element_type.109, bf16[128,512]{1,0:T(8,128)(2,1)S(1)} %slice.75, bf16[512,512]{1,0:T(8,128)(2,1)S(1)} %copy-done.5), kind=kOutput, calls=%fused_computation.15 | convolution fusion | flops 808583168 | bytes 3805184 | tf_op jit(solution)/shard_map/qhc,hcv->qhv/dot_general | solution.py:132
  65.1 0.8 copy.59
  66.0 2.1 %fusion.21 = bf16[2,2,512]{2,1,0:T(2,128)(2,1)S(1)} fusion(bf16[2,1024,512]{2,1,0:T(8,128)(2,1)} %param.29, f32[2,2,1024]{2,1,0:T(2,128)S(1)} %copy-done.16, f32[2,2]{1,0:T(2,128)S(1)} %copy-done.19, f32[2,512]{1,0:T(2,128)S(1)} %copy-done.17, f32[2,2]{1,0:T(2,128)S(1)} %copy-done.24), kind=kOutput, calls=%fused_computation.26 | convolution fusion | flops 4208640 | bytes 2121760 | tf_op jit(solution)/shard_map/bhk,bkc->bhc/dot_general | solution.py:169
  68.5 12.5 %reduce-scatter.9.cloned.1.call-done = bf16[128,2]{1,0:T(8,128)(2,1)} async-done(((bf16[512,2]{1,0:T(8,128)(2,1)}), bf16[128,2]{1,0:T(8,128)(2,1)}) %reduce-scatter.9.cloned.1.call-update) | async-done | bytes 528
  81.0 0.8 copy.62
  81.9 19.6 %reduce-scatter.7.cloned.1.call-done = bf16[128,256]{1,0:T(8,128)(2,1)} async-done(((bf16[512,256]{1,0:T(8,128)(2,1)}), bf16[128,256]{1,0:T(8,128)(2,1)}) %reduce-scatter.7.cloned.1.call-update) | async-done | bytes 65552
  101.5 0.9 copy.60
  102.5 10.9 %all_gather.3 = bf16[130,2048]{0,1:T(8,128)(2,1)S(1)} all-gather(bf16[130,256]{0,1:T(8,128)(2,1)S(1)} %pad_maximum_fusion.1), channel_id=1, replica_groups=mesh['kv'=4,'tp'=8] {'tp'}, dimensions={1}, use_global_device_ids=true | all-gather | bytes 599040 | tf_op jit(solution)/shard_map/all_gather | solution.py:189
  (118 shorter events, 14.7 us)
Async XLA Ops:
  7.2 9.9 %copy-start = (bf16[2048,512]{1,0:T(8,128)(2,1)S(1)}, bf16[2048,512]{1,0:T(8,128)(2,1)}, u32[]{:S(2)}) copy-start(bf16[2048,512]{1,0:T(8,128)(2,1)} %param.21) | copy-start | bytes 6291460
  7.2 73.9 %reduce-scatter.9.cloned.1.call-start = ((), (), s32[]{:S(2)}) async-start(), calls=%async_computation.3 | async-start | bytes 163840
  8.6 1.9 %copy-start.4 = (bf16[128,2048]{1,0:T(8,128)(2,1)S(1)}, bf16[128,2048]{1,0:T(8,128)(2,1)}, u32[]{:S(2)}) copy-start(bf16[128,2048]{1,0:T(8,128)(2,1)} %param.16) | copy-start | bytes 1572868
  8.6 1.9 %copy-start.20 = (bf16[2,2048]{1,0:T(2,128)(2,1)S(1)}, bf16[2,2048]{1,0:T(2,128)(2,1)}, u32[]{:S(2)}) copy-start(bf16[2,2048]{1,0:T(2,128)(2,1)} %param.17) | copy-start | bytes 24580
  8.7 1.9 %copy-start.26 = (bf16[2048,128]{1,0:T(8,128)(2,1)S(1)}, bf16[2048,128]{1,0:T(8,128)(2,1)}, u32[]{:S(2)}) copy-start(bf16[2048,128]{1,0:T(8,128)(2,1)} %param.20) | copy-start | bytes 1572868
  8.7 1.9 %copy-start.28 = (f32[2048]{0:T(1024)S(1)}, f32[2048]{0:T(1024)}, u32[]{:S(2)}) copy-start(f32[2048]{0:T(1024)} %param.18) | copy-start | bytes 24580
  11.0 5.9 %copy-start.2 = (bf16[2,128,512]{2,1,0:T(8,128)(2,1)S(1)}, bf16[2,128,512]{2,1,0:T(8,128)(2,1)}, u32[]{:S(2)}) copy-start(bf16[2,128,512]{2,1,0:T(8,128)(2,1)} %param.24) | copy-start | bytes 786436
  12.3 5.3 %copy-start.6 = (bf16[128,128]{1,0:T(8,128)(2,1)}, bf16[128,128]{1,0:T(8,128)(2,1)S(1)}, u32[]{:S(2)}) copy-start(bf16[128,128]{1,0:T(8,128)(2,1)S(1)} %copy.45) | copy-start | bytes 98308
  13.0 9.1 %collective-permute-start = (bf16[128,384]{1,0:T(8,128)(2,1)}, bf16[128,384]{1,0:T(8,128)(2,1)}, u32[]{:S(2)}, u32[]{:S(2)}) collective-permute-start(bf16[128,384]{1,0:T(8,128)(2,1)} %pad_maximum_fusion.2), channel_id=1, source_target_pairs={{0,8},{8,16},{16,24},{24,0},{1,9},{9,17},{17,25},{25,1},{2,10},{10... | collective-permute-start | bytes 294920 | tf_op jit(solution)/shard_map/ppermute | solution.py:111
  16.2 4.0 %copy-start.13 = (bf16[130,2,64]{2,1,0:T(2,128)(2,1)}, bf16[130,2,64]{2,1,0:T(2,128)(2,1)S(1)}, u32[]{:S(2)}) copy-start(bf16[130,2,64]{2,1,0:T(2,128)(2,1)S(1)} %pad_maximum_fusion.3) | copy-start | bytes 99844
  17.0 1.6 %copy-start.1 = (bf16[2,1024,512]{2,1,0:T(8,128)(2,1)S(1)}, bf16[2,1024,512]{2,1,0:T(8,128)(2,1)}, u32[]{:S(2)}) copy-start(bf16[2,1024,512]{2,1,0:T(8,128)(2,1)} %param.29) | copy-start | bytes 6291460
  17.7 1.8 %copy-start.27 = (bf16[2048,64]{0,1:T(8,128)(2,1)S(1)}, bf16[2048,64]{0,1:T(8,128)(2,1)}, u32[]{:S(2)}) copy-start(bf16[2048,64]{0,1:T(8,128)(2,1)} %param.22) | copy-start | bytes 786436
  21.9 1.8 %copy-start.15 = (f32[2,2,1024]{2,1,0:T(2,128)}, f32[2,2,1024]{2,1,0:T(2,128)S(1)}, u32[]{:S(2)}) copy-start(f32[2,2,1024]{2,1,0:T(2,128)S(1)} %get-tuple-element.13) | copy-start | bytes 49156
  21.9 20.5 %copy-start.5 = (bf16[512,512]{1,0:T(8,128)(2,1)S(1)}, bf16[512,512]{1,0:T(8,128)(2,1)}, u32[]{:S(2)}) copy-start(bf16[512,512]{1,0:T(8,128)(2,1)} %param.27) | copy-start | bytes 1572868
  21.9 1.8 %copy-start.18 = (f32[2,2]{1,0:T(2,128)}, f32[2,2]{1,0:T(2,128)S(1)}, u32[]{:S(2)}) copy-start(f32[2,2]{1,0:T(2,128)S(1)} %fusion.55) | copy-start | bytes 52
  22.1 6.7 %collective-permute-start.1 = (bf16[128,384]{1,0:T(8,128)(2,1)}, bf16[128,384]{1,0:T(8,128)(2,1)}, u32[]{:S(2)}, u32[]{:S(2)}) collective-permute-start(bf16[128,384]{1,0:T(8,128)(2,1)} %collective-permute-done), channel_id=1, source_target_pairs={{0,8},{8,16},{16,24},{24,0},{1,9},{9,17},{17,25},{25,1},{2,10},{10... | collective-permute-start | bytes 294920 | tf_op jit(solution)/shard_map/ppermute | solution.py:111
  28.8 6.6 %collective-permute-start.2 = (bf16[128,384]{1,0:T(8,128)(2,1)}, bf16[128,384]{1,0:T(8,128)(2,1)S(1)}, u32[]{:S(2)}, u32[]{:S(2)}) collective-permute-start(bf16[128,384]{1,0:T(8,128)(2,1)} %collective-permute-done.1), channel_id=1, source_target_pairs={{0,8},{8,16},{16,24},{24,0},{1,9},{9,17},{17,25},{25,1},{2,10},{10... | collective-permute-start | bytes 294920 | tf_op jit(solution)/shard_map/ppermute | solution.py:111
  42.4 3.7 %copy-start.7 = (bf16[512,128]{0,1:T(8,128)(2,1)S(1)}, bf16[512,128]{0,1:T(8,128)(2,1)}, u32[]{:S(2)}) copy-start(bf16[512,128]{0,1:T(8,128)(2,1)} %copy.47) | copy-start | bytes 393220
  42.4 3.7 %copy-start.14 = (bf16[512,64]{0,1:T(8,128)(2,1)S(1)}, bf16[512,64]{0,1:T(8,128)(2,1)}, u32[]{:S(2)}) copy-start(bf16[512,64]{0,1:T(8,128)(2,1)} %param.28) | copy-start | bytes 196612
  58.5 3.3 %copy-start.9 = (bf16[2,512,128]{2,1,0:T(8,128)(2,1)S(1)}, bf16[2,512,128]{2,1,0:T(8,128)(2,1)}, u32[]{:S(2)}) copy-start(bf16[2,512,128]{2,1,0:T(8,128)(2,1)} %param.25) | copy-start | bytes 786436
  61.7 39.8 %reduce-scatter.7.cloned.1.call-start = ((), (), s32[]{:S(2)}) async-start(), calls=%async_computation.2 | async-start | bytes 327680
  65.9 2.1 %copy-start.10 = (bf16[2,512,128]{2,1,0:T(8,128)(2,1)S(1)}, bf16[2,512,128]{2,1,0:T(8,128)(2,1)}, u32[]{:S(2)}) copy-start(bf16[2,512,128]{2,1,0:T(8,128)(2,1)} %param.25) | copy-start | bytes 786436
  65.9 2.3 %copy-start.21 = (f32[2,2]{1,0:T(2,128)S(1)}, f32[2,2]{1,0:T(2,128)}, u32[]{:S(2)}) copy-start(f32[2,2]{1,0:T(2,128)} %get-tuple-element.2) | copy-start | bytes 52
  68.0 45.4 %copy-start.3 = (bf16[2048,256]{1,0:T(8,128)(2,1)S(1)}, bf16[2048,256]{1,0:T(8,128)(2,1)}, u32[]{:S(2)}) copy-start(bf16[2048,256]{1,0:T(8,128)(2,1)} %param.26) | copy-start | bytes 3145732
  (10 other events, 8.7 us)
Sparse Core Ops, SparseCore 0:
  61.8 19.1 reduce-scatter.8
  83.3 18.1 reduce-scatter.6
